TPU v7x, 32 devices: a whole 2x2x4 slice. The times are simulated.
32 devices in a mesh: ep: 4 (over y, x), tp: 8 (over z, core).
Axes of the slice: x: 2, y: 2, z: 4, core: 2. Of those that a mesh axis runs over, the one named last changes fastest.
Arguments:
- tokens: bfloat16 [1024, 4096], P('ep'), may hold values from -6 to 6
- cotangent: bfloat16 [1024, 4096], P('ep'), may hold values from -6 to 6
- routing: int32 [1024, 2], P('ep'), may hold values from 0 to 3, all different within a row; in each aligned block of 256 rows (0 to 255, 256 to 511, ...) at most 160 rows name the same one
- group_gate: float32 [1024], P('ep'), may hold values from 0.2 to 1
- inner_gate: float32 [1024, 2], P('ep'), may hold values from 0.1 to 0.9
- w_gate: bfloat16 [4, 4096, 2048], P('ep', None, 'tp'), may hold values from -0.09375 to 0.09375
- w_up: bfloat16 [4, 4096, 2048], P('ep', None, 'tp'), may hold values from -0.09375 to 0.09375
- w_down: bfloat16 [4, 2048, 4096], P('ep', 'tp'), may hold values from -0.125 to 0.125
Outputs:
- token_grad: bfloat16 [1024, 4096], P('ep', 'tp')
- group_grad: float32 [1024], P('ep')
- inner_grad: float32 [1024, 2], P('ep')
- gate_weight_grad: bfloat16 [4, 4096, 2048], P('ep', None, 'tp')
- up_weight_grad: bfloat16 [4, 4096, 2048], P('ep', None, 'tp')
- down_weight_grad: bfloat16 [4, 2048, 4096], P('ep', 'tp')
Inputs may be any that keep to these rules, and one draw needn't show every extreme that they name: `routing`: each row names 2 different experts. Among the rows of one device (aligned blocks of 256 rows) no expert is named more than 160 times, and in every draw some expert is named exactly 160 times in some block.
All inputs are finite; a program needn't handle non-finite values.
Results may differ from a plain program's by a relative error of at most 0.02.
Values may be sent and summed in bfloat16 or wider, within the bound.
A program may use at most 128 MiB of HBM per device.

v0:
```python
import jax
import jax.numpy as jnp
from jax import lax
from jax.sharding import PartitionSpec as P


def per_device(tokens, cotangent, routing, group_gate, inner_gate, w_gate, w_up, w_down):
    expert_count = lax.axis_size("ep")
    tok_rows, model_width = tokens.shape
    top_k = routing.shape[1]
    capacity = tok_rows * top_k * 5 // (4 * expert_count)
    flat_route = routing.reshape(-1)
    one_hot = (flat_route[:, None] == jnp.arange(expert_count, dtype=jnp.int32)[None, :]).astype(
        jnp.int32
    )
    within = jnp.sum(one_hot * (jnp.cumsum(one_hot, axis=0) - 1), axis=1)
    slot_of = flat_route * capacity + within
    token_of = jnp.arange(tok_rows * top_k, dtype=jnp.int32) // top_k
    combine = (group_gate[:, None] * inner_gate).reshape(-1)
    send_weight = jnp.zeros((expert_count * capacity,), jnp.float32).at[slot_of].set(combine)

    def place_rows(source):
        empty = jnp.zeros((expert_count * capacity, source.shape[1]), source.dtype)
        return empty.at[slot_of].set(source[token_of])

    col_width = model_width // lax.axis_size("tp")
    offset = lax.axis_index("tp") * col_width
    token_cols = place_rows(lax.dynamic_slice_in_dim(tokens, offset, col_width, 1))
    cot_cols = place_rows(lax.dynamic_slice_in_dim(cotangent, offset, col_width, 1))
    token_cols, cot_cols, row_weight = (
        lax.all_to_all(token_cols, "ep", split_axis=0, concat_axis=0, tiled=True),
        lax.all_to_all(cot_cols, "ep", split_axis=0, concat_axis=0, tiled=True),
        lax.all_to_all(
            send_weight.astype(jnp.bfloat16), "ep", split_axis=0, concat_axis=0, tiled=True
        ).astype(send_weight.dtype),
    )
    rows_in, cot_rows = (
        lax.all_gather(token_cols, "tp", axis=1, tiled=True),
        lax.all_gather(cot_cols, "tp", axis=1, tiled=True),
    )
    gate_weight = w_gate[0]
    up_weight = w_up[0]
    down_weight = w_down[0]
    gate_pre = jnp.dot(rows_in, gate_weight, preferred_element_type=jnp.float32)
    up_pre = jnp.dot(rows_in, up_weight, preferred_element_type=jnp.float32)
    sigmoid_gate = jax.nn.sigmoid(gate_pre)
    silu_gate = gate_pre * sigmoid_gate
    hidden = (silu_gate * up_pre).astype(jnp.bfloat16)
    scaled_cot = (row_weight[:, None] * cot_rows).astype(jnp.bfloat16)
    down_grad = lax.dot_general(
        hidden, scaled_cot, (((0,), (0,)), ((), ())), preferred_element_type=jnp.float32
    )
    grad_hidden = lax.dot_general(
        cot_rows, down_weight, (((1,), (1,)), ((), ())), preferred_element_type=jnp.float32
    )
    partial_scores = jnp.sum(grad_hidden * hidden.astype(jnp.float32), axis=1)
    weighted = row_weight[:, None] * grad_hidden
    grad_gate_in = (
        weighted * up_pre * sigmoid_gate * (1.0 + gate_pre * (1.0 - sigmoid_gate))
    ).astype(jnp.bfloat16)
    grad_up_in = (weighted * silu_gate).astype(jnp.bfloat16)
    gate_grad = lax.dot_general(
        rows_in, grad_gate_in, (((0,), (0,)), ((), ())), preferred_element_type=jnp.float32
    )
    upper_grad = lax.dot_general(
        rows_in, grad_up_in, (((0,), (0,)), ((), ())), preferred_element_type=jnp.float32
    )
    partial_rows = lax.dot_general(
        grad_gate_in, gate_weight, (((1,), (1,)), ((), ())), preferred_element_type=jnp.float32
    ) + lax.dot_general(
        grad_up_in, up_weight, (((1,), (1,)), ((), ())), preferred_element_type=jnp.float32
    )
    row_grad = lax.psum_scatter(
        partial_rows.astype(jnp.bfloat16), "tp", scatter_dimension=1, tiled=True
    )
    scores = lax.psum(partial_scores, "tp")
    back_rows, back_scores = (
        lax.all_to_all(row_grad, "ep", split_axis=0, concat_axis=0, tiled=True),
        lax.all_to_all(
            scores.astype(jnp.bfloat16), "ep", split_axis=0, concat_axis=0, tiled=True
        ).astype(scores.dtype),
    )
    picked = back_rows[slot_of].astype(jnp.float32)
    token_grad = jnp.sum(picked.reshape(tok_rows, top_k, picked.shape[1]), axis=1).astype(
        jnp.bfloat16
    )
    score_of = back_scores[slot_of].reshape(tok_rows, top_k)
    inner_grad = group_gate[:, None] * score_of
    group_grad = jnp.sum(inner_gate * score_of, axis=1)
    return (
        token_grad,
        group_grad,
        inner_grad,
        gate_grad.astype(jnp.bfloat16)[None],
        upper_grad.astype(jnp.bfloat16)[None],
        down_grad.astype(jnp.bfloat16)[None],
    )


def solution(mesh):
    return jax.shard_map(
        per_device,
        mesh=mesh,
        in_specs=(
            P("ep", None),
            P("ep", None),
            P("ep", None),
            P("ep"),
            P("ep", None),
            P("ep", None, "tp"),
            P("ep", None, "tp"),
            P("ep", "tp", None),
        ),
        out_specs=(
            P("ep", "tp"),
            P("ep"),
            P("ep", None),
            P("ep", None, "tp"),
            P("ep", None, "tp"),
            P("ep", "tp", None),
        ),
        check_vma=False,
    )
```

profile of v0, /device:TPU:0, one launch (start us, length us, event | category | flops | bytes accessed | tf_op | source)
XLA Modules:
  0.0 238.5 jit_solution(333309969247349896)
XLA Ops:
  7.2 0.0 copy-start
  7.2 0.0 copy-start.4
  7.2 0.0 copy-start.3
  7.2 0.0 all-gather.5.cloned.1.call-start
  7.3 0.8 broadcast_multiply_fusion.2
  8.1 0.8 copy.21
  8.9 0.1 eq.29
  9.0 0.1 eq.25
  9.2 0.1 copy.20
  9.3 0.1 mul.81
  9.5 1.2 reduce-window.6
  10.7 0.2 slice_reduce_fusion
  11.0 0.2 reduce-window.9
  11.1 0.1 add_bitcast_fusion
  11.3 1.1 constant_dynamic-slice_fusion
  12.3 4.9 %scatter_custom_fusion.2 = bf16[640,512]{1,0:T(8,128)(2,1)S(1)} fusion(s32[512]{0:T(512)S(1)} %bitcast.64, bf16[256,512]{1,0:T(8,128)(2,1)S(1)} %get-tuple-element.24, s32[1024]{0:T(1024)S(1)} %pad_clamp_fusion.1, bf16[]{:T(256)} %constant.39.clone.1), kind=kCustom, calls=%fused_computation.32 | custom fusion | bytes 655362 | tf_op jit(solution)/shard_map/scatter | solution.py:24
  17.2 15.0 %all_to_all.56 = bf16[4,160,512]{2,1,0:T(8,128)(2,1)} all-to-all(bf16[4,160,512]{2,1,0:T(8,128)(2,1)S(1)} %bitcast.62), channel_id=1, replica_groups=mesh['ep'=4,'tp'=8] {'ep'}, dimensions={0} | all-to-all | bytes 1310720 | tf_op jit(solution)/shard_map/all_to_all | solution.py:31
  32.2 0.0 all-gather.5.cloned.1.call-update
  32.3 0.0 all-gather.3.cloned.1.call-start
  32.3 4.9 %scatter_custom_fusion.1 = bf16[640,512]{1,0:T(8,128)(2,1)S(1)} fusion(s32[512]{0:T(512)S(1)} %bitcast.65, bf16[256,512]{1,0:T(8,128)(2,1)S(1)} %get-tuple-element.25, s32[1024]{0:T(1024)S(1)} %pad_clamp_fusion.1, bf16[]{:T(256)} %constant.39.clone.1), kind=kCustom, calls=%fused_computation.34 | custom fusion | bytes 655362 | tf_op jit(solution)/shard_map/scatter | solution.py:24
  37.2 11.8 %all_to_all.57 = bf16[4,160,512]{2,1,0:T(8,128)(2,1)} all-to-all(bf16[4,160,512]{2,1,0:T(8,128)(2,1)S(1)} %bitcast.61), channel_id=1, replica_groups=mesh['ep'=4,'tp'=8] {'ep'}, dimensions={0} | all-to-all | bytes 1310720 | tf_op jit(solution)/shard_map/all_to_all | solution.py:32
  49.0 0.0 all-gather.3.cloned.1.call-update
  49.1 0.0 reduce-scatter.2.cloned.1.call-start
  49.1 0.0 copy-done.4
  49.1 0.1 copy.23
  49.3 0.0 copy-done.3
  49.3 0.1 broadcast_multiply_fusion.1
  49.4 0.1 reshape.172
  49.5 2.4 %scatter_custom_fusion = f32[640]{0:T(1024)S(1)} fusion(s32[512]{0:T(512)S(1)} %bitcast.66, f32[512]{0:T(512)S(1)} %reshape.172, f32[]{:T(128)} %constant.17.clone.1), kind=kCustom, calls=%fused_computation.59 | custom fusion | bytes 2564 | tf_op jit(solution)/shard_map/scatter | solution.py:20
  52.0 0.1 all_to_all.49
  52.1 7.0 %all_to_all.58 = bf16[4,160,1]{1,2,0:T(2,128)(2,1)S(1)} all-to-all(bf16[4,160,1]{1,2,0:T(2,128)(2,1)S(1)} %all_to_all.49), channel_id=1, replica_groups=mesh['ep'=4,'tp'=8] {'ep'}, dimensions={0} | all-to-all | bytes 2560 | tf_op jit(solution)/shard_map/all_to_all | solution.py:33
  59.1 0.1 reshape.134
  59.2 28.9 %all-gather.5.cloned.1.call-done = bf16[640,4096]{1,0:T(8,128)(2,1)} async-done(((bf16[640,512]{1,0:T(8,128)(2,1)}), bf16[640,4096]{1,0:T(8,128)(2,1)}) %all-gather.5.cloned.1.call-update) | async-done | bytes 5242896 | tf_op jit(solution)/shard_map/all_gather | solution.py:38
  88.1 0.0 copy-done
  88.1 0.0 copy-start.1
  88.1 5.3 %fusion.8 = f32[640,256]{0,1:T(8,128)} fusion(bf16[640,4096]{1,0:T(8,128)(2,1)} %all-gather.5.cloned.1.call-done, bf16[1,4096,256]{2,1,0:T(8,128)(2,1)S(1)} %copy-done), kind=kOutput, calls=%fused_computation.19 | convolution fusion | flops 1342177280 | bytes 7995392 | tf_op jit(solution)/shard_map/dot_general | solution.py:44
  93.4 0.0 copy-done.1
  93.4 0.0 copy-done.5
  93.4 2.8 %fusion.11 = f32[640,256]{0,1:T(8,128)} fusion(bf16[640,4096]{1,0:T(8,128)(2,1)S(1)} %copy-done.5, bf16[1,4096,256]{2,1,0:T(8,128)(2,1)S(1)} %copy-done.1), kind=kOutput, calls=%fused_computation.22 | convolution fusion | flops 1342177280 | bytes 7995392 | tf_op jit(solution)/shard_map/dot_general | solution.py:45
  96.3 48.2 %all-gather.3.cloned.1.call-done = bf16[640,4096]{1,0:T(8,128)(2,1)} async-done(((bf16[640,512]{1,0:T(8,128)(2,1)}), bf16[640,4096]{1,0:T(8,128)(2,1)}) %all-gather.3.cloned.1.call-update) | async-done | bytes 5242896 | tf_op jit(solution)/shard_map/all_gather | solution.py:39
  144.5 5.4 %multiply_reduce_fusion = (f32[640]{0:T(1024)S(1)}, bf16[640,256]{0,1:T(8,128)(2,1)S(1)}, bf16[640,256]{0,1:T(8,128)(2,1)S(1)}, bf16[640,256]{0,1:T(8,128)(2,1)S(1)}) fusion(f32[640,256]{0,1:T(8,128)} %fusion.11, f32[640,256]{0,1:T(8,128)} %fusion.8, f32[640]{0:T(1024)S(1)} %reshape.134, bf16[640,4096]{1,0:T(8,128)(2,1)} %all-gather.3.cloned.1.call-done, ...), kind=kOutput, calls=%fused_computation.26 | convolution fusion | flops 1345289600 | bytes 9638912 | tf_op jit(solution)/shard_map/dot_general | solution.py:53
  149.9 0.0 copy-start.2
  149.9 1.6 fusion.6
  151.5 0.0 copy-done.2
  151.5 4.1 %add_convert_fusion = bf16[640,4096]{1,0:T(8,128)(2,1)} fusion(f32[640,4096]{1,0:T(8,128)S(1)} %fusion.6, bf16[640,256]{0,1:T(8,128)(2,1)S(1)} %get-tuple-element.21, bf16[1,4096,256]{2,1,0:T(8,128)(2,1)S(1)} %copy-done.2), kind=kOutput, calls=%fused_computation.8 | convolution fusion | flops 1347420160 | bytes 18153472 | tf_op jit(solution)/shard_map/dot_general | solution.py:70
  155.6 0.0 reduce-scatter.2.cloned.1.call-update
  155.7 14.8 %psum.7 = bf16[640]{0:T(1024)(128)(2,1)S(1)} all-reduce(f32[640]{0:T(1024)S(1)} %get-tuple-element.18), channel_id=1, replica_groups=mesh['ep'=4,'tp'=8] {'tp'}, use_global_device_ids=true, to_apply=%region_9.10 | all-reduce | flops 640 | bytes 3840 | tf_op jit(solution)/shard_map/psum | solution.py:76
  170.5 0.7 all_to_all.50
  171.2 3.9 %all-to-all-start.4 = ((bf16[4,160,1]{1,2,0:T(2,128)(2,1)}), bf16[4,160,1]{1,2,0:T(2,128)(2,1)S(1)}, u32[]{:S(2)}, u32[]{:S(2)}) async-start(bf16[4,160,1]{1,2,0:T(2,128)(2,1)} %all_to_all.50), calls=%async_computation.5 | async-start | bytes 8192 | tf_op jit(solution)/shard_map/all_to_all | solution.py:79
  175.0 5.7 %fusion.5 = bf16[1,256,4096]{2,1,0:T(8,128)(2,1)} fusion(bf16[640,256]{0,1:T(8,128)(2,1)S(1)} %get-tuple-element.19, bf16[640,4096]{1,0:T(8,128)(2,1)} %all-gather.3.cloned.1.call-done, f32[640]{0:T(1024)S(1)} %reshape.134), kind=kOutput, calls=%fused_computation.16 | convolution fusion | flops 1351090176 | bytes 7670272 | tf_op jit(solution)/shard_map/dot_general | solution.py:50
  180.8 5.7 %fusion.3 = bf16[1,4096,256]{2,1,0:T(8,128)(2,1)} fusion(bf16[640,4096]{1,0:T(8,128)(2,1)} %all-gather.5.cloned.1.call-done, bf16[640,256]{0,1:T(8,128)(2,1)S(1)} %get-tuple-element.20), kind=kOutput, calls=%fused_computation.14 | convolution fusion | flops 1343225856 | bytes 7667712 | tf_op jit(solution)/shard_map/dot_general | solution.py:62
  186.5 0.0 all-to-all-done.4
  186.5 28.0 %reduce-scatter.2.cloned.1.call-done = bf16[640,512]{1,0:T(8,128)(2,1)} async-done(((bf16[640,4096]{1,0:T(8,128)(2,1)}), bf16[640,512]{1,0:T(8,128)(2,1)}) %reduce-scatter.2.cloned.1.call-update) | async-done | bytes 655376 | tf_op jit(solution)/shard_map/reduce_scatter | solution.py:73
  214.5 3.6 %all-to-all-start.3 = ((bf16[4,160,512]{2,1,0:T(8,128)(2,1)}), bf16[4,160,512]{2,1,0:T(8,128)(2,1)S(1)}, u32[]{:S(2)}, u32[]{:S(2)}) async-start(bf16[4,160,512]{2,1,0:T(8,128)(2,1)} %bitcast.63), calls=%async_computation.4 | async-start | bytes 1310720 | tf_op jit(solution)/shard_map/all_to_all | solution.py:78
  218.2 5.7 %fusion.4 = bf16[1,4096,256]{2,1,0:T(8,128)(2,1)} fusion(bf16[640,4096]{1,0:T(8,128)(2,1)} %all-gather.5.cloned.1.call-done, bf16[640,256]{0,1:T(8,128)(2,1)S(1)} %get-tuple-element.21), kind=kOutput, calls=%fused_computation.15 | convolution fusion | flops 1343225856 | bytes 7667712 | tf_op jit(solution)/shard_map/dot_general | solution.py:65
  223.8 0.1 reshape.135
  223.9 2.3 gather_fusion.1
  226.2 0.1 reshape.133
  226.4 0.7 broadcast_multiply_fusion
  227.0 0.7 copy.27
  227.7 0.0 all-to-all-done.3
  227.7 2.0 gather_fusion
  229.7 0.2 gather.17
  229.9 2.1 reduce_sum.43
  (10 shorter events, 0.1 us)
Async XLA Ops:
  7.2 81.0 %copy-start = (bf16[1,4096,256]{2,1,0:T(8,128)(2,1)S(1)}, bf16[1,4096,256]{2,1,0:T(8,128)(2,1)}, u32[]{:S(2)}) copy-start(bf16[1,4096,256]{2,1,0:T(8,128)(2,1)} %param.13) | copy-start | bytes 6291460
  7.2 41.9 %copy-start.4 = (f32[256,2]{0,1:T(2,128)S(1)}, f32[256,2]{0,1:T(2,128)}, u32[]{:S(2)}) copy-start(f32[256,2]{0,1:T(2,128)} %param.12) | copy-start | bytes 6148
  7.2 42.1 %copy-start.3 = (f32[256]{0:T(256)S(1)}, f32[256]{0:T(256)}, u32[]{:S(2)}) copy-start(f32[256]{0:T(256)} %param.11) | copy-start | bytes 3076
  7.2 80.9 %all-gather.5.cloned.1.call-start = ((), (), s32[]{:S(2)}) async-start(), calls=%async_computation.7 | async-start | bytes 5898240 | tf_op jit(solution)/shard_map/all_gather | solution.py:38
  32.3 112.2 %all-gather.3.cloned.1.call-start = ((), (), s32[]{:S(2)}) async-start(), calls=%async_computation.6 | async-start | bytes 5898240 | tf_op jit(solution)/shard_map/all_gather | solution.py:39
  49.1 165.4 %reduce-scatter.2.cloned.1.call-start = ((), (), s32[]{:S(2)}) async-start(), calls=%async_computation.8 | async-start | bytes 5898240 | tf_op jit(solution)/shard_map/reduce_scatter | solution.py:73
  88.1 5.3 %copy-start.1 = (bf16[1,4096,256]{2,1,0:T(8,128)(2,1)S(1)}, bf16[1,4096,256]{2,1,0:T(8,128)(2,1)}, u32[]{:S(2)}) copy-start(bf16[1,4096,256]{2,1,0:T(8,128)(2,1)} %param.14) | copy-start | bytes 6291460
  88.1 5.3 %copy-start.5 = (bf16[640,4096]{1,0:T(8,128)(2,1)S(1)}, bf16[640,4096]{1,0:T(8,128)(2,1)}, u32[]{:S(2)}) copy-start(bf16[640,4096]{1,0:T(8,128)(2,1)} %all-gather.5.cloned.1.call-done) | copy-start | bytes 15728644
  149.9 1.6 copy-start.2
  171.2 15.3 %all-to-all-start.4 = ((bf16[4,160,1]{1,2,0:T(2,128)(2,1)}), bf16[4,160,1]{1,2,0:T(2,128)(2,1)S(1)}, u32[]{:S(2)}, u32[]{:S(2)}) async-start(bf16[4,160,1]{1,2,0:T(2,128)(2,1)} %all_to_all.50), calls=%async_computation.5 | async-start | bytes 8192 | tf_op jit(solution)/shard_map/all_to_all | solution.py:79
  214.5 13.2 %all-to-all-start.3 = ((bf16[4,160,512]{2,1,0:T(8,128)(2,1)}), bf16[4,160,512]{2,1,0:T(8,128)(2,1)S(1)}, u32[]{:S(2)}, u32[]{:S(2)}) async-start(bf16[4,160,512]{2,1,0:T(8,128)(2,1)} %bitcast.63), calls=%async_computation.4 | async-start | bytes 1310720 | tf_op jit(solution)/shard_map/all_to_all | solution.py:78
Sparse Core Ops, SparseCore 0:
  32.4 55.6 all-gather.4
  89.7 54.7 all-gather.2
  155.8 58.7 reduce-scatter.1
where the time goes:
time: 239 us; the launch traced here: 238 us
  waiting for transfers between devices  105 us (44%)
  blocking collectives  48.7 us (20%)
  matrix products  36.3 us (15%)
  local copies, waits for them, and re-layouts  21.4 us (9%)
  between operations  14 us (6%)
  starting transfers between devices  7.63 us (3%)
  other arithmetic  5.27 us (2%)
    all_gather x1, waiting for transfers between devices, per_device(): lax.all_gather(cot_cols, 'tp', axis=1, tiled=True)  48.2 us
    all_gather x1, waiting for transfers between devices, per_device(): lax.all_gather(token_cols, 'tp', axis=1, tiled=True)  28.9 us
    reduce_scatter x1, waiting for transfers between devices, per_device(): lax.psum_scatter(partial_rows.astype(jnp.bfloat16), 'tp', scatter_dimensi...  28 us
    all_to_all x1, blocking collectives, per_device(): lax.all_to_all(token_cols, 'ep', split_axis=0, concat_axis=0, tiled=True)  15 us
    psum x1, blocking collectives, per_device(): scores = lax.psum(partial_scores, 'tp')  14.8 us
    all_to_all x1, blocking collectives, per_device(): lax.all_to_all(cot_cols, 'ep', split_axis=0, concat_axis=0, tiled=True)  11.8 us
    scatter x2, local copies, waits for them, and re-layouts, place_rows(): return empty.at[slot_of].set(source[token_of])  9.78 us
    all_to_all x1, blocking collectives, per_device(): lax.all_to_all(send_weight.astype(jnp.bfloat16), 'ep', split_axis=0, conc...  7.01 us
  transfers between devices with their start and end apart: 5, of which 3 were waited for; matrix products, arithmetic and copies ran while one was open for 15% of the time, Pallas kernels for 0%

commit v1 on v0

--- a/solution.py
+++ b/solution.py
@@ -73,7 +73,7 @@
     row_grad = lax.psum_scatter(
         partial_rows.astype(jnp.bfloat16), "tp", scatter_dimension=1, tiled=True
     )
-    scores = lax.psum(partial_scores, "tp")
+    scores = jnp.sum(lax.all_gather(partial_scores, "tp"), axis=0)
     back_rows, back_scores = (
         lax.all_to_all(row_grad, "ep", split_axis=0, concat_axis=0, tiled=True),
         lax.all_to_all(

time: 239 us -> 240 us (level)
    psum x1 -> x0, blocking collectives: 14.8 us -> none  [per_device(): scores = lax.psum(partial_scores, 'tp')]
    all_gather x0 -> x1, blocking collectives: none -> 14.2 us  [per_device(): scores = jnp.sum(lax.all_gather(partial_scores, 'tp'), axis=0)]
  transfers between devices with their start and end apart: 5 -> 5, of which waited for: 3 -> 3; matrix products, arithmetic and copies ran while one was open for 15% -> 16% of each run, Pallas kernels for 0% -> 0%
where the time goes in v1:
time: 240 us; the launch traced here: 239 us
  waiting for transfers between devices  106 us (44%)
  blocking collectives  48.1 us (20%)
  matrix products  37.2 us (16%)
  local copies, waits for them, and re-layouts  21.4 us (9%)
  between operations  14 us (6%)
  starting transfers between devices  7.42 us (3%)
  other arithmetic  5.3 us (2%)
    all_gather x1, waiting for transfers between devices, per_device(): lax.all_gather(cot_cols, 'tp', axis=1, tiled=True)  48.2 us
    all_gather x1, waiting for transfers between devices, per_device(): lax.all_gather(token_cols, 'tp', axis=1, tiled=True)  28.9 us
    reduce_scatter x1, waiting for transfers between devices, per_device(): lax.psum_scatter(partial_rows.astype(jnp.bfloat16), 'tp', scatter_dimensi...  28.6 us
    all_to_all x1, blocking collectives, per_device(): lax.all_to_all(token_cols, 'ep', split_axis=0, concat_axis=0, tiled=True)  15 us
    all_gather x1, blocking collectives, per_device(): scores = jnp.sum(lax.all_gather(partial_scores, 'tp'), axis=0)  14.2 us
    all_to_all x1, blocking collectives, per_device(): lax.all_to_all(cot_cols, 'ep', split_axis=0, concat_axis=0, tiled=True)  11.8 us
    scatter x2, local copies, waits for them, and re-layouts, place_rows(): return empty.at[slot_of].set(source[token_of])  9.78 us
    all_to_all x1, blocking collectives, per_device(): lax.all_to_all(send_weight.astype(jnp.bfloat16), 'ep', split_axis=0, conc...  7.01 us
  transfers between devices with their start and end apart: 5, of which 3 were waited for; matrix products, arithmetic and copies ran while one was open for 16% of the time, Pallas kernels for 0%

profile of v1, /device:TPU:0, one launch (start us, length us, event | category | flops | bytes accessed | tf_op | source)
XLA Modules:
  0.0 239.1 jit_solution(16147345241928082204)
XLA Ops:
  7.2 0.0 copy-start
  7.2 0.0 copy-start.4
  7.2 0.0 copy-start.3
  7.2 0.0 all-gather.7.cloned.1.call-start
  7.3 0.8 broadcast_multiply_fusion.2
  8.1 0.8 copy.21
  8.9 0.1 eq.29
  9.0 0.1 eq.25
  9.2 0.1 copy.20
  9.3 0.1 mul.81
  9.5 1.2 reduce-window.6
  10.7 0.2 slice_reduce_fusion
  11.0 0.2 reduce-window.9
  11.1 0.1 add_bitcast_fusion
  11.3 1.1 constant_dynamic-slice_fusion
  12.3 4.9 %scatter_custom_fusion.2 = bf16[640,512]{1,0:T(8,128)(2,1)S(1)} fusion(s32[512]{0:T(512)S(1)} %bitcast.64, bf16[256,512]{1,0:T(8,128)(2,1)S(1)} %get-tuple-element.24, s32[1024]{0:T(1024)S(1)} %pad_clamp_fusion.1, bf16[]{:T(256)} %constant.39.clone.1), kind=kCustom, calls=%fused_computation.32 | custom fusion | bytes 655362 | tf_op jit(solution)/shard_map/scatter | solution.py:24
  17.2 15.0 %all_to_all.52 = bf16[4,160,512]{2,1,0:T(8,128)(2,1)} all-to-all(bf16[4,160,512]{2,1,0:T(8,128)(2,1)S(1)} %bitcast.62), channel_id=1, replica_groups=mesh['ep'=4,'tp'=8] {'ep'}, dimensions={0} | all-to-all | bytes 1310720 | tf_op jit(solution)/shard_map/all_to_all | solution.py:31
  32.2 0.0 all-gather.7.cloned.1.call-update
  32.3 0.0 all-gather.5.cloned.1.call-start
  32.3 4.9 %scatter_custom_fusion.1 = bf16[640,512]{1,0:T(8,128)(2,1)S(1)} fusion(s32[512]{0:T(512)S(1)} %bitcast.65, bf16[256,512]{1,0:T(8,128)(2,1)S(1)} %get-tuple-element.25, s32[1024]{0:T(1024)S(1)} %pad_clamp_fusion.1, bf16[]{:T(256)} %constant.39.clone.1), kind=kCustom, calls=%fused_computation.34 | custom fusion | bytes 655362 | tf_op jit(solution)/shard_map/scatter | solution.py:24
  37.2 11.8 %all_to_all.53 = bf16[4,160,512]{2,1,0:T(8,128)(2,1)} all-to-all(bf16[4,160,512]{2,1,0:T(8,128)(2,1)S(1)} %bitcast.61), channel_id=1, replica_groups=mesh['ep'=4,'tp'=8] {'ep'}, dimensions={0} | all-to-all | bytes 1310720 | tf_op jit(solution)/shard_map/all_to_all | solution.py:32
  49.0 0.0 all-gather.5.cloned.1.call-update
  49.1 0.0 reduce-scatter.2.cloned.1.call-start
  49.1 0.0 copy-done.4
  49.1 0.1 copy.23
  49.3 0.0 copy-done.3
  49.3 0.1 broadcast_multiply_fusion.1
  49.4 0.1 reshape.183
  49.5 2.4 %scatter_custom_fusion = f32[640]{0:T(1024)S(1)} fusion(s32[512]{0:T(512)S(1)} %bitcast.66, f32[512]{0:T(512)S(1)} %reshape.183, f32[]{:T(128)} %constant.17.clone.1), kind=kCustom, calls=%fused_computation.59 | custom fusion | bytes 2564 | tf_op jit(solution)/shard_map/scatter | solution.py:20
  52.0 0.1 all_to_all.46
  52.1 7.0 %all_to_all.54 = bf16[4,160,1]{1,2,0:T(2,128)(2,1)S(1)} all-to-all(bf16[4,160,1]{1,2,0:T(2,128)(2,1)S(1)} %all_to_all.46), channel_id=1, replica_groups=mesh['ep'=4,'tp'=8] {'ep'}, dimensions={0} | all-to-all | bytes 2560 | tf_op jit(solution)/shard_map/all_to_all | solution.py:33
  59.1 0.1 reshape.145
  59.2 28.9 %all-gather.7.cloned.1.call-done = bf16[640,4096]{1,0:T(8,128)(2,1)} async-done(((bf16[640,512]{1,0:T(8,128)(2,1)}), bf16[640,4096]{1,0:T(8,128)(2,1)}) %all-gather.7.cloned.1.call-update) | async-done | bytes 5242896 | tf_op jit(solution)/shard_map/all_gather | solution.py:38
  88.1 0.0 copy-done
  88.1 0.0 copy-start.1
  88.1 0.0 copy-start.5
  88.1 5.3 %fusion.8 = f32[640,256]{0,1:T(8,128)} fusion(bf16[640,4096]{1,0:T(8,128)(2,1)} %all-gather.7.cloned.1.call-done, bf16[1,4096,256]{2,1,0:T(8,128)(2,1)S(1)} %copy-done), kind=kOutput, calls=%fused_computation.19 | convolution fusion | flops 1342177280 | bytes 7995392 | tf_op jit(solution)/shard_map/dot_general | solution.py:44
  93.4 0.0 copy-done.1
  93.4 0.0 copy-done.5
  93.4 2.8 %fusion.11 = f32[640,256]{0,1:T(8,128)} fusion(bf16[640,4096]{1,0:T(8,128)(2,1)S(1)} %copy-done.5, bf16[1,4096,256]{2,1,0:T(8,128)(2,1)S(1)} %copy-done.1), kind=kOutput, calls=%fused_computation.22 | convolution fusion | flops 1342177280 | bytes 7995392 | tf_op jit(solution)/shard_map/dot_general | solution.py:45
  96.3 48.2 %all-gather.5.cloned.1.call-done = bf16[640,4096]{1,0:T(8,128)(2,1)} async-done(((bf16[640,512]{1,0:T(8,128)(2,1)}), bf16[640,4096]{1,0:T(8,128)(2,1)}) %all-gather.5.cloned.1.call-update) | async-done | bytes 5242896 | tf_op jit(solution)/shard_map/all_gather | solution.py:39
  144.5 6.1 %multiply_reduce_fusion = (f32[640]{0:T(1024)S(1)}, bf16[640,256]{0,1:T(8,128)(2,1)}, bf16[640,256]{0,1:T(8,128)(2,1)S(1)}, bf16[640,256]{0,1:T(8,128)(2,1)S(1)}) fusion(f32[640,256]{0,1:T(8,128)} %fusion.11, f32[640,256]{0,1:T(8,128)} %fusion.8, f32[640]{0:T(1024)S(1)} %reshape.145, bf16[640,4096]{1,0:T(8,128)(2,1)} %all-gather.5.cloned.1.call-done, ...), kind=kOutput, calls=%fused_computation.26 | convolution fusion | flops 1345289600 | bytes 9638912 | tf_op jit(solution)/shard_map/dot_general | solution.py:53
  150.6 1.6 fusion.6
  152.2 0.0 copy-done.2
  152.2 4.1 %add_convert_fusion = bf16[640,4096]{1,0:T(8,128)(2,1)} fusion(f32[640,4096]{1,0:T(8,128)S(1)} %fusion.6, bf16[640,256]{0,1:T(8,128)(2,1)S(1)} %get-tuple-element.21, bf16[1,4096,256]{2,1,0:T(8,128)(2,1)S(1)} %copy-done.2), kind=kOutput, calls=%fused_computation.8 | convolution fusion | flops 1347420160 | bytes 18153472 | tf_op jit(solution)/shard_map/dot_general | solution.py:70
  156.3 0.0 reduce-scatter.2.cloned.1.call-update
  156.4 14.2 %all-gather.1 = f32[8,1,640]{2,1,0:T(1,128)S(1)} all-gather(f32[1,1,640]{2,1,0:T(1,128)S(1)} %reshape.204), channel_id=2, replica_groups=mesh['ep'=4,'tp'=8] {'tp'}, dimensions={0}, use_global_device_ids=true | all-gather | bytes 23040 | tf_op jit(solution)/shard_map/all_gather | solution.py:76
  170.6 0.7 convert_element_type.90
  171.3 3.6 %all-to-all-start.4 = ((bf16[4,160,1]{1,2,0:T(2,128)(2,1)}), bf16[4,160,1]{1,2,0:T(2,128)(2,1)S(1)}, u32[]{:S(2)}, u32[]{:S(2)}) async-start(bf16[4,160,1]{1,2,0:T(2,128)(2,1)} %convert_element_type.90), calls=%async_computation.5 | async-start | bytes 8192 | tf_op jit(solution)/shard_map/all_to_all | solution.py:79
  174.9 5.9 %fusion.5 = bf16[1,256,4096]{2,1,0:T(8,128)(2,1)} fusion(bf16[640,256]{0,1:T(8,128)(2,1)} %get-tuple-element.19, bf16[640,4096]{1,0:T(8,128)(2,1)} %all-gather.5.cloned.1.call-done, f32[640]{0:T(1024)S(1)} %reshape.145), kind=kOutput, calls=%fused_computation.16 | convolution fusion | flops 1351090176 | bytes 7670272 | tf_op jit(solution)/shard_map/dot_general | solution.py:50
  180.8 5.7 %fusion.3 = bf16[1,4096,256]{2,1,0:T(8,128)(2,1)} fusion(bf16[640,4096]{1,0:T(8,128)(2,1)} %all-gather.7.cloned.1.call-done, bf16[640,256]{0,1:T(8,128)(2,1)S(1)} %get-tuple-element.20), kind=kOutput, calls=%fused_computation.14 | convolution fusion | flops 1343225856 | bytes 7667712 | tf_op jit(solution)/shard_map/dot_general | solution.py:62
  186.5 0.0 all-to-all-done.4
  186.5 28.6 %reduce-scatter.2.cloned.1.call-done = bf16[640,512]{1,0:T(8,128)(2,1)} async-done(((bf16[640,4096]{1,0:T(8,128)(2,1)}), bf16[640,512]{1,0:T(8,128)(2,1)}) %reduce-scatter.2.cloned.1.call-update) | async-done | bytes 655376 | tf_op jit(solution)/shard_map/reduce_scatter | solution.py:73
  215.1 3.7 %all-to-all-start.3 = ((bf16[4,160,512]{2,1,0:T(8,128)(2,1)}), bf16[4,160,512]{2,1,0:T(8,128)(2,1)S(1)}, u32[]{:S(2)}, u32[]{:S(2)}) async-start(bf16[4,160,512]{2,1,0:T(8,128)(2,1)} %bitcast.63), calls=%async_computation.4 | async-start | bytes 1310720 | tf_op jit(solution)/shard_map/all_to_all | solution.py:78
  218.8 5.7 %fusion.4 = bf16[1,4096,256]{2,1,0:T(8,128)(2,1)} fusion(bf16[640,4096]{1,0:T(8,128)(2,1)} %all-gather.7.cloned.1.call-done, bf16[640,256]{0,1:T(8,128)(2,1)S(1)} %get-tuple-element.21), kind=kOutput, calls=%fused_computation.15 | convolution fusion | flops 1343225856 | bytes 7667712 | tf_op jit(solution)/shard_map/dot_general | solution.py:65
  224.5 0.1 reshape.146
  224.6 2.3 gather_fusion.1
  226.9 0.1 reshape.144
  227.0 0.7 broadcast_multiply_fusion
  227.7 0.7 copy.27
  228.3 0.0 all-to-all-done.3
  228.4 2.0 gather_fusion
  230.3 0.2 gather.17
  230.5 2.1 reduce_sum.52
  (12 shorter events, 0.1 us)
Async XLA Ops:
  7.2 81.0 %copy-start = (bf16[1,4096,256]{2,1,0:T(8,128)(2,1)S(1)}, bf16[1,4096,256]{2,1,0:T(8,128)(2,1)}, u32[]{:S(2)}) copy-start(bf16[1,4096,256]{2,1,0:T(8,128)(2,1)} %param.13) | copy-start | bytes 6291460
  7.2 41.9 %copy-start.4 = (f32[256,2]{0,1:T(2,128)S(1)}, f32[256,2]{0,1:T(2,128)}, u32[]{:S(2)}) copy-start(f32[256,2]{0,1:T(2,128)} %param.12) | copy-start | bytes 6148
  7.2 42.1 %copy-start.3 = (f32[256]{0:T(256)S(1)}, f32[256]{0:T(256)}, u32[]{:S(2)}) copy-start(f32[256]{0:T(256)} %param.11) | copy-start | bytes 3076
  7.2 80.9 %all-gather.7.cloned.1.call-start = ((), (), s32[]{:S(2)}) async-start(), calls=%async_computation.7 | async-start | bytes 5898240 | tf_op jit(solution)/shard_map/all_gather | solution.py:38
  32.3 112.2 %all-gather.5.cloned.1.call-start = ((), (), s32[]{:S(2)}) async-start(), calls=%async_computation.6 | async-start | bytes 5898240 | tf_op jit(solution)/shard_map/all_gather | solution.py:39
  49.1 166.1 %reduce-scatter.2.cloned.1.call-start = ((), (), s32[]{:S(2)}) async-start(), calls=%async_computation.8 | async-start | bytes 5898240 | tf_op jit(solution)/shard_map/reduce_scatter | solution.py:73
  88.1 5.3 %copy-start.1 = (bf16[1,4096,256]{2,1,0:T(8,128)(2,1)S(1)}, bf16[1,4096,256]{2,1,0:T(8,128)(2,1)}, u32[]{:S(2)}) copy-start(bf16[1,4096,256]{2,1,0:T(8,128)(2,1)} %param.14) | copy-start | bytes 6291460
  88.1 5.3 %copy-start.5 = (bf16[640,4096]{1,0:T(8,128)(2,1)S(1)}, bf16[640,4096]{1,0:T(8,128)(2,1)}, u32[]{:S(2)}) copy-start(bf16[640,4096]{1,0:T(8,128)(2,1)} %all-gather.7.cloned.1.call-done) | copy-start | bytes 15728644
  150.6 1.6 copy-start.2
  171.3 15.2 %all-to-all-start.4 = ((bf16[4,160,1]{1,2,0:T(2,128)(2,1)}), bf16[4,160,1]{1,2,0:T(2,128)(2,1)S(1)}, u32[]{:S(2)}, u32[]{:S(2)}) async-start(bf16[4,160,1]{1,2,0:T(2,128)(2,1)} %convert_element_type.90), calls=%async_computation.5 | async-start | bytes 8192 | tf_op jit(solution)/shard_map/all_to_all | solution.py:79
  215.1 13.2 %all-to-all-start.3 = ((bf16[4,160,512]{2,1,0:T(8,128)(2,1)}), bf16[4,160,512]{2,1,0:T(8,128)(2,1)S(1)}, u32[]{:S(2)}, u32[]{:S(2)}) async-start(bf16[4,160,512]{2,1,0:T(8,128)(2,1)} %bitcast.63), calls=%async_computation.4 | async-start | bytes 1310720 | tf_op jit(solution)/shard_map/all_to_all | solution.py:78
Sparse Core Ops, SparseCore 0:
  32.4 55.6 all-gather.6
  89.7 54.7 all-gather.4
  156.5 58.6 reduce-scatter.1
